TPU v7x, 32 devices: a whole 2x2x4 slice. The times are simulated.
32 devices in a mesh: ep: 4 (over y, x), tp: 8 (over z, core).
Axes of the slice: x: 2, y: 2, z: 4, core: 2. Of those that a mesh axis runs over, the one named last changes fastest.
Arguments:
- tokens: bfloat16 [64, 2048], P('ep', 'tp'), may hold values from -6 to 6
- key_cache: bfloat16 [64, 16, 1024, 128], P('ep', 'tp'), may hold values from -1700 to 1700
- value_cache: bfloat16 [64, 16, 1024, 128], P('ep', 'tp'), may hold values from -6 to 6
- gate_totals: float32 [64, 16, 1024], P('ep', 'tp'), as said below
- lengths: int32 [64], P('ep'), may hold values from 128 to 1024
- attn_gain: float32 [2048], replicated, may hold values from 0.1 to 1.9
- w_query: bfloat16 [2048, 2048], P(None, 'tp'), may hold values from -0.125 to 0.125
- w_key: bfloat16 [2048, 2048], P(None, 'tp'), may hold values from -0.125 to 0.125
- w_value: bfloat16 [2048, 2048], P(None, 'tp'), may hold values from -0.125 to 0.125
- w_forget: bfloat16 [2048, 16], replicated, may hold values from -0.125 to 0.125
- forget_bias: float32 [16], replicated, may hold values from -3 to 0
- w_attn_out: bfloat16 [2048, 2048], P('tp'), may hold values from -0.1875 to 0.1875
- moe_gain: float32 [2048], replicated, may hold values from 0.1 to 1.9
- group_ids: int32 [64, 1], P('ep'), may hold values from 0 to 3; in each aligned block of 16 rows (0 to 15, 16 to 31, ...) at most 8 rows name the same one
- inner_ids: int32 [64, 2], P('ep'), may hold values from 0 to 3, all different within a row
- group_prob: float32 [64], P('ep'), may hold values from 0.2 to 1
- pair_logits: float32 [64, 2], P('ep'), may hold values from -6 to 6
- w_expert_gate: bfloat16 [4, 2048, 2048], P('ep', None, 'tp'), may hold values from -0.125 to 0.125
- w_expert_up: bfloat16 [4, 2048, 2048], P('ep', None, 'tp'), may hold values from -0.125 to 0.125
- w_expert_down: bfloat16 [4, 2048, 2048], P('ep', 'tp'), may hold values from -0.375 to 0.375
- w_dense_in: bfloat16 [2048, 2048], P(None, 'tp'), may hold values from -0.125 to 0.125
- w_dense_out: bfloat16 [2048, 2048], P('tp'), may hold values from -0.1875 to 0.1875
- dense_gate: float32 [2048], P('tp'), may hold values from -2 to 2
Outputs:
- layer_output: bfloat16 [64, 2048], P('ep', 'tp')
- new_keys: bfloat16 [64, 16, 128], P('ep', 'tp')
- new_values: bfloat16 [64, 16, 128], P('ep', 'tp')
- new_gates: float32 [64, 16], P('ep', 'tp')
Inputs may be any that keep to these rules, and one draw needn't show every extreme that they name: `group_ids`: within the 16 sequences of each index of ep (aligned blocks of rows), no group is named by more than 8 sequences, a bound that some block reaches. `inner_ids`: each row names 2 different experts of its group. `gate_totals`: along positions the values of each sequence and head never rise.
All inputs are finite; a program needn't handle non-finite values.
Results may differ from a plain program's by a relative error of at most 0.011.
Values may be sent and summed in bfloat16 or wider, within the bound.
No kernel may reach another device: no remote copies, remote signals or barrier semaphores. Data moves between devices by JAX's collectives and lax.ppermute only.
A program may use at most 64 MiB of HBM per device.

v0:
```python
import jax
import jax.numpy as jnp
from jax import lax
from jax.sharding import PartitionSpec as P

FFE = 512
EPG = 4


EPS = 1e-06
FLOOR = -1e30


def norm_rows(row_data, gain_vec):
    values = row_data.astype(jnp.float32)
    factor = lax.rsqrt(jnp.mean(values * values, axis=-1, keepdims=True) + EPS)
    return (values * factor * gain_vec).astype(jnp.bfloat16)


def head_norm(values):
    factor = lax.rsqrt(jnp.mean(values * values, axis=-1, keepdims=True) + EPS)
    return (values * factor).astype(jnp.bfloat16)


def attend(queries, fresh_key, fresh_value, key_cache, value_cache, gate_totals, lengths, current):
    score_scale = queries.shape[-1] ** (-0.5)
    scores = (
        jnp.einsum("shd,shld->shl", queries, key_cache, preferred_element_type=jnp.float32)
        * score_scale
    )
    scores = scores + current[:, :, None] - gate_totals
    entry_indices = jnp.arange(key_cache.shape[2])
    live_mask = (entry_indices[None, :] < lengths[:, None])[:, None, :]
    scores = jnp.where(live_mask, scores, FLOOR)
    own_score = (
        jnp.sum(queries.astype(jnp.float32) * fresh_key.astype(jnp.float32), axis=-1) * score_scale
    )
    peak = jnp.maximum(jnp.max(scores, axis=-1), own_score)
    expo_terms = jnp.where(live_mask, jnp.exp(scores - peak[:, :, None]), 0.0)
    own_expo = jnp.exp(own_score - peak)
    denom_sum = jnp.sum(expo_terms, axis=-1) + own_expo
    weights = (expo_terms / denom_sum[:, :, None]).astype(jnp.bfloat16)
    own_weight = (own_expo / denom_sum).astype(jnp.bfloat16)
    attended = jnp.einsum("shl,shld->shd", weights, value_cache, preferred_element_type=jnp.float32)
    attended = attended + own_weight.astype(jnp.float32)[:, :, None] * fresh_value.astype(
        jnp.float32
    )
    return attended.astype(jnp.bfloat16)


def body(
    tokens,
    key_cache,
    value_cache,
    gate_totals,
    lengths,
    attn_gain,
    w_query,
    w_key,
    w_value,
    w_forget,
    forget_bias,
    w_attn_out,
    moe_gain,
    group_ids,
    inner_ids,
    group_prob,
    pair_logits,
    w_expert_gate,
    w_expert_up,
    w_expert_down,
    w_dense_in,
    w_dense_out,
    dense_gate,
):
    gathered = lax.all_gather(tokens, "tp", axis=1, tiled=True)
    normed = norm_rows(gathered, attn_gain)
    seq_count = gathered.shape[0]
    heads_dev = key_cache.shape[1]
    head_dim = key_cache.shape[3]

    def project(weight):
        return jnp.dot(normed, weight, preferred_element_type=jnp.float32).reshape(
            seq_count, heads_dev, head_dim
        )

    queries = head_norm(project(w_query))
    new_keys = head_norm(project(w_key))
    new_values = project(w_value).astype(jnp.bfloat16)
    first_head = lax.axis_index("tp") * heads_dev
    forget_cols = lax.dynamic_slice_in_dim(w_forget, first_head, heads_dev, 1)
    forget_shift = lax.dynamic_slice_in_dim(forget_bias, first_head, heads_dev, 0)
    log_gate = jax.nn.log_sigmoid(
        jnp.dot(normed, forget_cols, preferred_element_type=jnp.float32) + forget_shift
    )
    entry_indices = jnp.arange(gate_totals.shape[2])
    at_last = (entry_indices[None, :] == (lengths - 1)[:, None])[:, None, :]
    new_gates = jnp.sum(jnp.where(at_last, gate_totals, 0.0), axis=2) + log_gate
    attended = attend(
        queries, new_keys, new_values, key_cache, value_cache, gate_totals, lengths, new_gates
    )
    partial_value = jnp.dot(
        attended.reshape(seq_count, heads_dev * head_dim),
        w_attn_out,
        preferred_element_type=jnp.float32,
    )
    piece_sum = lax.psum_scatter(partial_value, "tp", scatter_dimension=1, tiled=True)
    own_residual = (tokens.astype(jnp.float32) + piece_sum).astype(jnp.bfloat16)
    moe_in = norm_rows(lax.all_gather(own_residual, "tp", axis=1, tiled=True), moe_gain)
    groups = lax.axis_size("ep")
    capacity = max(2, 2 * seq_count // groups)
    first_share = jax.nn.sigmoid(pair_logits[:, 0] - pair_logits[:, 1])
    pair_share = group_prob[:, None] * jnp.stack([first_share, 1.0 - first_share], axis=1)
    inner_range = jnp.arange(EPG)
    spread = jnp.sum(
        jnp.where(inner_ids[:, :, None] == inner_range[None, None, :], pair_share[:, :, None], 0.0),
        axis=1,
    ).astype(jnp.bfloat16)
    choose = (group_ids == jnp.arange(groups)[None, :]).astype(jnp.int32)
    before = jnp.cumsum(choose, axis=0) - choose
    slot_of = group_ids[:, 0] * capacity + jnp.sum(before * choose, axis=1)
    slot_ids = jnp.arange(groups * capacity)
    send_map = (slot_of[None, :] == slot_ids[:, None]).astype(jnp.bfloat16)
    send_weights = jnp.dot(send_map, spread, preferred_element_type=jnp.float32).astype(
        jnp.bfloat16
    )
    send_rows = jnp.dot(send_map, moe_in, preferred_element_type=jnp.float32).astype(jnp.bfloat16)
    recv_rows, recv_weights = (
        lax.all_to_all(send_rows, "ep", split_axis=0, concat_axis=0, tiled=True),
        lax.all_to_all(send_weights, "ep", split_axis=0, concat_axis=0, tiled=True),
    )
    dense_hidden = jax.nn.silu(
        jnp.dot(moe_in, w_dense_in, preferred_element_type=jnp.float32)
    ).astype(jnp.bfloat16)
    dense_part = jnp.dot(dense_hidden, w_dense_out, preferred_element_type=jnp.float32)
    hidden_dev = w_expert_gate.shape[2]
    expert_index = lax.axis_index("tp") * hidden_dev // FFE
    route_col = jnp.sum(
        jnp.where(inner_range[None, :] == expert_index, recv_weights.astype(jnp.float32), 0.0),
        axis=1,
    )
    gate_pre = jnp.dot(recv_rows, w_expert_gate[0], preferred_element_type=jnp.float32)
    up_pre = jnp.dot(recv_rows, w_expert_up[0], preferred_element_type=jnp.float32)
    hidden = (jax.nn.silu(gate_pre) * up_pre * route_col[:, None]).astype(jnp.bfloat16)
    expert_part = jnp.dot(hidden, w_expert_down[0], preferred_element_type=jnp.float32)
    expert_sum, dense_sum = (
        lax.psum_scatter(expert_part, "tp", scatter_dimension=1, tiled=True),
        lax.psum_scatter(dense_part, "tp", scatter_dimension=1, tiled=True),
    )
    returned = lax.all_to_all(
        expert_sum.astype(jnp.bfloat16), "ep", split_axis=0, concat_axis=0, tiled=True
    )
    expert_out = lax.dot_general(
        send_map, returned, (((0,), (0,)), ((), ())), preferred_element_type=jnp.float32
    )
    layer_output = (
        own_residual.astype(jnp.float32) + expert_out + jax.nn.sigmoid(dense_gate) * dense_sum
    )
    return (layer_output.astype(jnp.bfloat16), new_keys, new_values, new_gates)


def solution(mesh):
    placed = (
        P("ep", "tp"),
        P("ep", "tp", None, None),
        P("ep", "tp", None, None),
        P("ep", "tp", None),
        P("ep"),
        P(),
        P(None, "tp"),
        P(None, "tp"),
        P(None, "tp"),
        P(),
        P(),
        P("tp", None),
        P(),
        P("ep", None),
        P("ep", None),
        P("ep"),
        P("ep", None),
        P("ep", None, "tp"),
        P("ep", None, "tp"),
        P("ep", "tp", None),
        P(None, "tp"),
        P("tp", None),
        P("tp"),
    )
    return jax.shard_map(
        body,
        mesh=mesh,
        in_specs=placed,
        out_specs=(P("ep", "tp"), P("ep", "tp", None), P("ep", "tp", None), P("ep", "tp")),
        check_vma=False,
    )
```

profile of v0, /device:TPU:0, one launch (start us, length us, event | category | flops | bytes accessed | tf_op | source)
XLA Modules:
  0.0 172.8 jit_solution(14352880859179264883)
XLA Ops:
  7.2 0.0 copy-start
  7.2 0.0 copy-start.5
  7.2 0.0 copy-start.4
  7.2 0.0 reduce-scatter.4.cloned.1.call-start
  7.3 0.8 broadcast_add_fusion
  8.1 0.7 iota_compare_fusion.1
  8.8 15.9 %all_gather.6 = bf16[16,2048]{1,0:T(8,128)(2,1)S(1)} all-gather(bf16[16,256]{1,0:T(8,128)(2,1)} %param.23), channel_id=1, replica_groups=mesh['ep'=4,'tp'=8] {'tp'}, dimensions={1}, use_global_device_ids=true | all-gather | bytes 73728 | tf_op jit(solution)/shard_map/all_gather | solution.py:76
  24.7 0.1 fusion.12
  24.8 1.5 fusion.67
  26.4 0.1 multiply_reduce_fusion.1
  26.5 1.5 fusion.70
  28.0 0.1 multiply_reduce_fusion.2
  28.1 0.1 iota_compare_fusion
  28.2 1.1 select_reduce_fusion
  29.3 0.1 copy.45
  29.4 0.7 dynamic_slice.7
  30.1 1.0 fusion.58
  31.1 0.0 copy-start.11
  31.1 0.1 copy.46
  31.2 0.7 multiply_reduce_fusion
  31.9 5.6 %fusion.34 = f32[16,2,1,1024]{3,2,1,0:T(1,128)S(1)} fusion(bf16[16,2,1024,128]{3,2,1,0:T(8,128)(2,1)} %param.24, bf16[16,2,128,1]{2,1,0,3:T(2,128)(2,1)S(1)} %get-tuple-element.12), kind=kOutput, calls=%fused_computation.48 | convolution fusion | flops 8388608 | bytes 8527872 | tf_op jit(solution)/shard_map/shd,shld->shl/dot_general | solution.py:28
  37.6 0.0 copy-start.14
  37.6 0.0 copy-start.10
  37.6 0.0 copy-start.8
  37.6 0.0 copy-start.6
  37.6 0.3 fusion.72
  37.9 0.3 fusion.32
  38.2 0.3 fusion.26
  38.5 0.3 convolution_convert_fusion.1
  38.8 0.0 copy-start.7
  38.8 0.0 copy-start.1
  38.8 0.0 copy-start.2
  38.9 0.0 copy-start.13
  38.9 4.7 %fusion.24 = f32[16,2,1,128]{3,2,1,0:T(1,128)S(1)} fusion(bf16[16,2,1024,128]{3,2,1,0:T(8,128)(2,1)} %param.25, bf16[16,2,1024,1]{2,1,0,3:T(2,128)(2,1)S(1)} %fusion.26), kind=kOutput, calls=%fused_computation.33 | convolution fusion | flops 8388608 | bytes 8470528 | tf_op jit(solution)/shard_map/shl,shld->shd/dot_general | solution.py:44
  43.6 0.1 add_convert_fusion.1
  43.7 2.1 %fusion.46 = f32[16,2048]{1,0:T(8,128)} fusion(bf16[256,2048]{1,0:T(8,128)(2,1)} %param.34, bf16[2,8,2,128]{3,2,1,0:T(2,128)(2,1)S(1)} %bitcast.56), kind=kOutput, calls=%fused_computation.66 | convolution fusion | flops 16777216 | bytes 1187840 | tf_op jit(solution)/shard_map/dot_general | solution.py:102
  45.8 0.0 reduce-scatter.4.cloned.1.call-update
  45.8 0.1 fusion.53
  45.9 0.2 select_reduce_fusion.2
  46.2 0.1 convolution_convert_fusion.2
  46.3 0.1 all_to_all.25
  46.4 0.6 copy.49
  47.0 3.7 %all-to-all-start.1 = ((bf16[4,8,4]{1,2,0:T(4,128)(2,1)}), bf16[4,8,4]{1,2,0:T(4,128)(2,1)S(1)}, u32[]{:S(2)}, u32[]{:S(2)}) async-start(bf16[4,8,4]{1,2,0:T(4,128)(2,1)} %copy.49), calls=%async_computation.2 | async-start | bytes 8192 | tf_op jit(solution)/shard_map/all_to_all | solution.py:130
  50.8 26.8 %reduce-scatter.4.cloned.1.call-done = f32[16,256]{1,0:T(8,128)} async-done(((f32[16,2048]{1,0:T(8,128)}), f32[16,256]{1,0:T(8,128)}) %reduce-scatter.4.cloned.1.call-update) | async-done | bytes 16400 | tf_op jit(solution)/shard_map/reduce_scatter | solution.py:107
  77.6 0.7 add_convert_fusion
  78.3 13.9 %all_gather.7 = bf16[16,2048]{1,0:T(8,128)(2,1)S(1)} all-gather(bf16[16,256]{1,0:T(8,128)(2,1)S(1)} %add_convert_fusion), channel_id=1, replica_groups=mesh['ep'=4,'tp'=8] {'tp'}, dimensions={1}, use_global_device_ids=true | all-gather | bytes 73728 | tf_op jit(solution)/shard_map/all_gather | solution.py:109
  92.2 0.1 fusion.15
  92.4 0.9 fusion
  93.2 3.6 %all-to-all-start = ((bf16[4,8,2048]{2,1,0:T(8,128)(2,1)}), bf16[4,8,2048]{2,1,0:T(8,128)(2,1)S(1)}, u32[]{:S(2)}, u32[]{:S(2)}) async-start(bf16[4,8,2048]{2,1,0:T(8,128)(2,1)} %fusion), calls=%async_computation.1 | async-start | bytes 262144 | tf_op jit(solution)/shard_map/all_to_all | solution.py:129
  96.9 0.1 select_reduce_fusion.1
  97.0 0.1 mul.181
  97.1 4.8 %all-to-all-done = bf16[4,8,2048]{2,1,0:T(8,128)(2,1)S(1)} async-done(((bf16[4,8,2048]{2,1,0:T(8,128)(2,1)}), bf16[4,8,2048]{2,1,0:T(8,128)(2,1)S(1)}, u32[]{:S(2)}, u32[]{:S(2)}) %all-to-all-start) | async-done | bytes 131104 | tf_op jit(solution)/shard_map/all_to_all | solution.py:129
  101.9 1.5 fusion.10
  103.4 0.0 copy-done
  103.4 2.7 %fusion.4 = f32[32,2048]{1,0:T(8,128)} fusion(bf16[1,256,2048]{2,1,0:T(8,128)(2,1)S(1)} %copy-done, bf16[1,2048,256]{2,1,0:T(8,128)(2,1)} %param.41, bf16[4,8,2048]{2,1,0:T(8,128)(2,1)S(1)} %all-to-all-done, f32[32,256]{1,0:T(8,128)S(1)} %fusion.10, f32[32]{0:T(128)S(1)} %mul.181), kind=kOutput, calls=%fused_computation.7 | convolution fusion | flops 67166208 | bytes 2523264 | tf_op jit(solution)/shard_map/dot_general | solution.py:145
  106.1 0.0 reduce-scatter.6.cloned.1.call-update
  106.1 0.0 reduce-scatter.8.cloned.1.call-start
  106.2 1.5 fusion.44
  107.6 0.0 reduce-scatter.8.cloned.1.call-update
  107.7 26.1 %reduce-scatter.6.cloned.1.call-done = f32[32,256]{1,0:T(8,128)} async-done(((f32[32,2048]{1,0:T(8,128)}), f32[32,256]{1,0:T(8,128)}) %reduce-scatter.6.cloned.1.call-update) | async-done | bytes 32784 | tf_op jit(solution)/shard_map/reduce_scatter | solution.py:147
  133.7 1.4 convert_bitcast_fusion
  135.1 3.6 %all-to-all-start.2 = ((bf16[4,8,256]{2,1,0:T(8,128)(2,1)}), bf16[4,8,256]{2,1,0:T(8,128)(2,1)S(1)}, u32[]{:S(2)}, u32[]{:S(2)}) async-start(bf16[4,8,256]{2,1,0:T(8,128)(2,1)} %convert_bitcast_fusion), calls=%async_computation.4 | async-start | bytes 32768 | tf_op jit(solution)/shard_map/all_to_all | solution.py:150
  138.7 26.0 %reduce-scatter.8.cloned.1.call-done = f32[16,256]{1,0:T(8,128)} async-done(((f32[16,2048]{1,0:T(8,128)}), f32[16,256]{1,0:T(8,128)}) %reduce-scatter.8.cloned.1.call-update) | async-done | bytes 16400 | tf_op jit(solution)/shard_map/reduce_scatter | solution.py:148
  164.7 1.5 fusion.5
  (35 shorter events, 0.2 us)
Async XLA Ops:
  7.2 96.2 %copy-start = (bf16[1,256,2048]{2,1,0:T(8,128)(2,1)S(1)}, bf16[1,256,2048]{2,1,0:T(8,128)(2,1)}, u32[]{:S(2)}) copy-start(bf16[1,256,2048]{2,1,0:T(8,128)(2,1)} %param.42) | copy-start | bytes 3145732
  7.2 31.3 %copy-start.5 = (f32[2048]{0:T(1024)S(1)}, f32[2048]{0:T(1024)}, u32[]{:S(2)}) copy-start(f32[2048]{0:T(1024)} %param.28) | copy-start | bytes 24580
  7.2 30.3 %copy-start.4 = (f32[16,2,1024]{2,1,0:T(2,128)S(1)}, f32[16,2,1024]{2,1,0:T(2,128)}, u32[]{:S(2)}) copy-start(f32[16,2,1024]{2,1,0:T(2,128)} %param.26) | copy-start | bytes 393220
  7.2 31.3 %copy-start.3 = (bf16[2048,256]{1,0:T(8,128)(2,1)S(1)}, bf16[2048,256]{1,0:T(8,128)(2,1)}, u32[]{:S(2)}) copy-start(bf16[2048,256]{1,0:T(8,128)(2,1)} %param.31) | copy-start | bytes 3145732
  7.2 70.3 %reduce-scatter.4.cloned.1.call-start = ((), (), s32[]{:S(2)}) async-start(), calls=%async_computation.6 | async-start | bytes 147456 | tf_op jit(solution)/shard_map/reduce_scatter | solution.py:107
  31.1 12.5 %copy-start.11 = (f32[16,2]{0,1:T(2,128)}, f32[16,2]{0,1:T(2,128)S(1)}, u32[]{:S(2)}) copy-start(f32[16,2]{0,1:T(2,128)S(1)} %fusion.58) | copy-start | bytes 388
  37.5 8.3 %copy-start.9 = (s32[16,1]{0,1:T(1,128)S(1)}, s32[16,1]{0,1:T(1,128)}, u32[]{:S(2)}) copy-start(s32[16,1]{0,1:T(1,128)} %param.36) | copy-start | bytes 196
  37.5 8.6 %copy-start.12 = (f32[16,2]{0,1:T(2,128)S(1)}, f32[16,2]{0,1:T(2,128)}, u32[]{:S(2)}) copy-start(f32[16,2]{0,1:T(2,128)} %param.39) | copy-start | bytes 388
  37.6 8.6 %copy-start.14 = (f32[16]{0:T(128)S(1)}, f32[16]{0:T(128)}, u32[]{:S(2)}) copy-start(f32[16]{0:T(128)} %param.38) | copy-start | bytes 196
  37.6 8.6 %copy-start.10 = (s32[16,2]{0,1:T(2,128)S(1)}, s32[16,2]{0,1:T(2,128)}, u32[]{:S(2)}) copy-start(s32[16,2]{0,1:T(2,128)} %param.37) | copy-start | bytes 388
  37.6 40.0 %copy-start.8 = (bf16[16,256]{1,0:T(8,128)(2,1)S(1)}, bf16[16,256]{1,0:T(8,128)(2,1)}, u32[]{:S(2)}) copy-start(bf16[16,256]{1,0:T(8,128)(2,1)} %param.23) | copy-start | bytes 24580
  37.6 54.8 %copy-start.6 = (f32[2048]{0:T(1024)S(1)}, f32[2048]{0:T(1024)}, u32[]{:S(2)}) copy-start(f32[2048]{0:T(1024)} %param.35) | copy-start | bytes 24580
  38.8 67.3 %copy-start.7 = (bf16[16,2,128]{2,1,0:T(2,128)(2,1)}, bf16[16,2,128]{2,1,0:T(2,128)(2,1)S(1)}, u32[]{:S(2)}) copy-start(bf16[16,2,128]{2,1,0:T(2,128)(2,1)S(1)} %convert_element_type.102) | copy-start | bytes 24580
  38.8 67.3 %copy-start.1 = (bf16[256,2048]{1,0:T(8,128)(2,1)S(1)}, bf16[256,2048]{1,0:T(8,128)(2,1)}, u32[]{:S(2)}) copy-start(bf16[256,2048]{1,0:T(8,128)(2,1)} %param.44) | copy-start | bytes 3145732
  38.8 67.3 %copy-start.2 = (bf16[2048,256]{1,0:T(8,128)(2,1)S(1)}, bf16[2048,256]{1,0:T(8,128)(2,1)}, u32[]{:S(2)}) copy-start(bf16[2048,256]{1,0:T(8,128)(2,1)} %param.43) | copy-start | bytes 3145732
  38.9 99.9 %copy-start.13 = (f32[256]{0:T(256)S(1)}, f32[256]{0:T(256)}, u32[]{:S(2)}) copy-start(f32[256]{0:T(256)} %param.45) | copy-start | bytes 3076
  47.0 46.2 %all-to-all-start.1 = ((bf16[4,8,4]{1,2,0:T(4,128)(2,1)}), bf16[4,8,4]{1,2,0:T(4,128)(2,1)S(1)}, u32[]{:S(2)}, u32[]{:S(2)}) async-start(bf16[4,8,4]{1,2,0:T(4,128)(2,1)} %copy.49), calls=%async_computation.2 | async-start | bytes 8192 | tf_op jit(solution)/shard_map/all_to_all | solution.py:130
  93.2 8.7 %all-to-all-start = ((bf16[4,8,2048]{2,1,0:T(8,128)(2,1)}), bf16[4,8,2048]{2,1,0:T(8,128)(2,1)S(1)}, u32[]{:S(2)}, u32[]{:S(2)}) async-start(bf16[4,8,2048]{2,1,0:T(8,128)(2,1)} %fusion), calls=%async_computation.1 | async-start | bytes 262144 | tf_op jit(solution)/shard_map/all_to_all | solution.py:129
  96.9 36.9 %reduce-scatter.6.cloned.1.call-start = ((), (), s32[]{:S(2)}) async-start(), calls=%async_computation.7 | async-start | bytes 294912 | tf_op jit(solution)/shard_map/reduce_scatter | solution.py:147
  106.1 58.6 %reduce-scatter.8.cloned.1.call-start = ((), (), s32[]{:S(2)}) async-start(), calls=%async_computation.8 | async-start | bytes 147456 | tf_op jit(solution)/shard_map/reduce_scatter | solution.py:148
  135.1 29.6 %all-to-all-start.2 = ((bf16[4,8,256]{2,1,0:T(8,128)(2,1)}), bf16[4,8,256]{2,1,0:T(8,128)(2,1)S(1)}, u32[]{:S(2)}, u32[]{:S(2)}) async-start(bf16[4,8,256]{2,1,0:T(8,128)(2,1)} %convert_bitcast_fusion), calls=%async_computation.4 | async-start | bytes 32768 | tf_op jit(solution)/shard_map/all_to_all | solution.py:150
Sparse Core Ops, SparseCore 0:
  45.9 31.5 reduce-scatter.3
  106.2 27.4 reduce-scatter.5
  136.0 28.7 reduce-scatter.7
where the time goes:
time: 174 us; the launch traced here: 173 us
  waiting for transfers between devices  83.8 us (48%)
  blocking collectives  29.8 us (17%)
  matrix products  24.9 us (14%)
  between operations  14 us (8%)
  starting transfers between devices  11 us (6%)
  other arithmetic  7.35 us (4%)
  local copies, waits for them, and re-layouts  1.82 us (1%)
    reduce_scatter x1, waiting for transfers between devices, body(): lax.psum_scatter(partial_value, 'tp', scatter_dimension=1, tiled=True)  26.8 us
    reduce_scatter x1, waiting for transfers between devices, body(): lax.psum_scatter(expert_part, 'tp', scatter_dimension=1, tiled=True)  26.1 us
    reduce_scatter x1, waiting for transfers between devices, body(): lax.psum_scatter(dense_part, 'tp', scatter_dimension=1, tiled=True)  26 us
    all_gather x1, blocking collectives, body(): gathered = lax.all_gather(tokens, 'tp', axis=1, tiled=True)  15.9 us
    all_gather x1, blocking collectives, body(): lax.all_gather(own_residual, 'tp', axis=1, tiled=True)  13.9 us
    dot_general x1, matrix products, attend(): jnp.einsum('shd,shld->shl', queries, key_cache, preferred_element_type=jn...  5.63 us
    all_to_all x1, waiting for transfers between devices, body(): lax.all_to_all(send_rows, 'ep', split_axis=0, concat_axis=0, tiled=True)  4.85 us
    dot_general x1, matrix products, attend(): jnp.einsum('shl,shld->shd', weights, value_cache, preferred_element_type=...  4.72 us
  transfers between devices with their start and end apart: 6, of which 4 were waited for; matrix products, arithmetic and copies ran while one was open for 3% of the time, Pallas kernels for 0%

commit v1 on v0

--- a/solution.py
+++ b/solution.py
@@ -73,11 +73,30 @@
     w_dense_out,
     dense_gate,
 ):
-    gathered = lax.all_gather(tokens, "tp", axis=1, tiled=True)
-    normed = norm_rows(gathered, attn_gain)
-    seq_count = gathered.shape[0]
+    tp_size = lax.axis_size("tp")
+    groups = lax.axis_size("ep")
+    seq_count, width = tokens.shape
+    model_dim = width * tp_size
     heads_dev = key_cache.shape[1]
     head_dim = key_cache.shape[3]
+
+    gate_high = lax.reduce_precision(dense_gate, 8, 7)
+    gate_low = dense_gate - gate_high
+    gate_rows = jnp.pad(jnp.stack([gate_high, gate_low]), ((0, 6), (0, 0))).astype(jnp.bfloat16)
+    own_block = jnp.concatenate([tokens, gate_rows], axis=0)
+    first_recv = lax.all_to_all(
+        jnp.broadcast_to(own_block, (tp_size,) + own_block.shape),
+        "tp",
+        split_axis=0,
+        concat_axis=0,
+        tiled=True,
+    )
+    gathered = first_recv[:, :seq_count].transpose(1, 0, 2).reshape(seq_count, model_dim)
+    full_gate = (
+        first_recv[:, seq_count].astype(jnp.float32)
+        + first_recv[:, seq_count + 1].astype(jnp.float32)
+    ).reshape(model_dim)
+    normed = norm_rows(gathered, attn_gain)
 
     def project(weight):
         return jnp.dot(normed, weight, preferred_element_type=jnp.float32).reshape(
@@ -88,11 +107,8 @@
     new_keys = head_norm(project(w_key))
     new_values = project(w_value).astype(jnp.bfloat16)
     first_head = lax.axis_index("tp") * heads_dev
-    forget_cols = lax.dynamic_slice_in_dim(w_forget, first_head, heads_dev, 1)
-    forget_shift = lax.dynamic_slice_in_dim(forget_bias, first_head, heads_dev, 0)
-    log_gate = jax.nn.log_sigmoid(
-        jnp.dot(normed, forget_cols, preferred_element_type=jnp.float32) + forget_shift
-    )
+    forget_all = jnp.dot(normed, w_forget, preferred_element_type=jnp.float32) + forget_bias
+    log_gate = jax.nn.log_sigmoid(lax.dynamic_slice_in_dim(forget_all, first_head, heads_dev, 1))
     entry_indices = jnp.arange(gate_totals.shape[2])
     at_last = (entry_indices[None, :] == (lengths - 1)[:, None])[:, None, :]
     new_gates = jnp.sum(jnp.where(at_last, gate_totals, 0.0), axis=2) + log_gate
@@ -103,11 +119,17 @@
         attended.reshape(seq_count, heads_dev * head_dim),
         w_attn_out,
         preferred_element_type=jnp.float32,
-    )
-    piece_sum = lax.psum_scatter(partial_value, "tp", scatter_dimension=1, tiled=True)
+    ).astype(jnp.bfloat16)
+    pieces = lax.all_to_all(
+        partial_value.reshape(seq_count, tp_size, width).transpose(1, 0, 2),
+        "tp",
+        split_axis=0,
+        concat_axis=0,
+        tiled=True,
+    )
+    piece_sum = jnp.sum(pieces.astype(jnp.float32), axis=0)
     own_residual = (tokens.astype(jnp.float32) + piece_sum).astype(jnp.bfloat16)
-    moe_in = norm_rows(lax.all_gather(own_residual, "tp", axis=1, tiled=True), moe_gain)
-    groups = lax.axis_size("ep")
+
     capacity = max(2, 2 * seq_count // groups)
     first_share = jax.nn.sigmoid(pair_logits[:, 0] - pair_logits[:, 1])
     pair_share = group_prob[:, None] * jnp.stack([first_share, 1.0 - first_share], axis=1)
@@ -121,41 +143,52 @@
     slot_of = group_ids[:, 0] * capacity + jnp.sum(before * choose, axis=1)
     slot_ids = jnp.arange(groups * capacity)
     send_map = (slot_of[None, :] == slot_ids[:, None]).astype(jnp.bfloat16)
-    send_weights = jnp.dot(send_map, spread, preferred_element_type=jnp.float32).astype(
-        jnp.bfloat16
-    )
-    send_rows = jnp.dot(send_map, moe_in, preferred_element_type=jnp.float32).astype(jnp.bfloat16)
-    recv_rows, recv_weights = (
-        lax.all_to_all(send_rows, "ep", split_axis=0, concat_axis=0, tiled=True),
-        lax.all_to_all(send_weights, "ep", split_axis=0, concat_axis=0, tiled=True),
-    )
-    dense_hidden = jax.nn.silu(
-        jnp.dot(moe_in, w_dense_in, preferred_element_type=jnp.float32)
-    ).astype(jnp.bfloat16)
-    dense_part = jnp.dot(dense_hidden, w_dense_out, preferred_element_type=jnp.float32)
+    row_data = jnp.concatenate([own_residual, jnp.pad(spread, ((0, 0), (0, 128 - EPG)))], axis=1)
+    send_rows = jnp.dot(send_map, row_data, preferred_element_type=jnp.float32).astype(jnp.bfloat16)
+    wide = row_data.shape[1]
+    send_blocks = jnp.broadcast_to(
+        send_rows.reshape(groups, 1, capacity, wide), (groups, tp_size, capacity, wide)
+    ).reshape(groups * tp_size, capacity, wide)
+    recv_blocks = lax.all_to_all(
+        send_blocks, ("ep", "tp"), split_axis=0, concat_axis=0, tiled=True
+    ).reshape(groups, tp_size, capacity, wide)
+    recv_rows = (
+        recv_blocks[..., :width].transpose(0, 2, 1, 3).reshape(groups * capacity, model_dim)
+    )
+    recv_weights = recv_blocks[:, 0, :, width : width + EPG].reshape(groups * capacity, EPG)
+    moe_in = norm_rows(recv_rows, moe_gain)
     hidden_dev = w_expert_gate.shape[2]
     expert_index = lax.axis_index("tp") * hidden_dev // FFE
     route_col = jnp.sum(
         jnp.where(inner_range[None, :] == expert_index, recv_weights.astype(jnp.float32), 0.0),
         axis=1,
     )
-    gate_pre = jnp.dot(recv_rows, w_expert_gate[0], preferred_element_type=jnp.float32)
-    up_pre = jnp.dot(recv_rows, w_expert_up[0], preferred_element_type=jnp.float32)
+    dense_hidden = jax.nn.silu(
+        jnp.dot(moe_in, w_dense_in, preferred_element_type=jnp.float32)
+    ).astype(jnp.bfloat16)
+    gate_pre = jnp.dot(moe_in, w_expert_gate[0], preferred_element_type=jnp.float32)
+    up_pre = jnp.dot(moe_in, w_expert_up[0], preferred_element_type=jnp.float32)
     hidden = (jax.nn.silu(gate_pre) * up_pre * route_col[:, None]).astype(jnp.bfloat16)
+    dense_part = jnp.dot(dense_hidden, w_dense_out, preferred_element_type=jnp.float32)
     expert_part = jnp.dot(hidden, w_expert_down[0], preferred_element_type=jnp.float32)
-    expert_sum, dense_sum = (
-        lax.psum_scatter(expert_part, "tp", scatter_dimension=1, tiled=True),
-        lax.psum_scatter(dense_part, "tp", scatter_dimension=1, tiled=True),
-    )
+    both = (expert_part + jax.nn.sigmoid(full_gate) * dense_part).astype(jnp.bfloat16)
     returned = lax.all_to_all(
-        expert_sum.astype(jnp.bfloat16), "ep", split_axis=0, concat_axis=0, tiled=True
-    )
-    expert_out = lax.dot_general(
-        send_map, returned, (((0,), (0,)), ((), ())), preferred_element_type=jnp.float32
-    )
-    layer_output = (
-        own_residual.astype(jnp.float32) + expert_out + jax.nn.sigmoid(dense_gate) * dense_sum
-    )
+        both.reshape(groups, capacity, tp_size, width)
+        .transpose(0, 2, 1, 3)
+        .reshape(groups * tp_size, capacity, width),
+        ("ep", "tp"),
+        split_axis=0,
+        concat_axis=0,
+        tiled=True,
+    ).reshape(groups * tp_size * capacity, width)
+    take_map = jnp.broadcast_to(
+        send_map.reshape(groups, 1, capacity, seq_count),
+        (groups, tp_size, capacity, seq_count),
+    ).reshape(groups * tp_size * capacity, seq_count)
+    branch_sum = lax.dot_general(
+        take_map, returned, (((0,), (0,)), ((), ())), preferred_element_type=jnp.float32
+    )
+    layer_output = own_residual.astype(jnp.float32) + branch_sum
     return (layer_output.astype(jnp.bfloat16), new_keys, new_values, new_gates)
 
 

time: 174 us -> 79.9 us (0.46)
  waiting for transfers between devices: 83.8 us -> 21.4 us
  blocking collectives: 29.8 us -> 0 us
  between operations: 14 us -> 0.92 us
  local copies, waits for them, and re-layouts: 1.82 us -> 10.8 us
  matrix products: 24.9 us -> 18.3 us
  starting transfers between devices: 11 us -> 17.2 us
  other arithmetic: 7.35 us -> 10.5 us
    reduce_scatter x3 -> x0, waiting for transfers between devices: 78.9 us -> none  [the longest x1 26.8 us: body(): lax.psum_scatter(partial_value, 'tp', scatter_dimension=1, tiled=True)]
    all_gather x2 -> x0, blocking collectives: 29.8 us -> none  [the longest x1 15.9 us: body(): gathered = lax.all_gather(tokens, 'tp', axis=1, tiled=True)]
    all_to_all x3 -> x4, waiting for transfers between devices: 4.85 us -> 21.4 us  [the longest x1 8.76 us: body(): lax.all_to_all(send_blocks, ('ep', 'tp'), split_axis=0, concat_axis=0, ti...]
    all_to_all x3 -> x4, starting transfers between devices: 11 us -> 17.2 us  [the longest x1 6.35 us: body(): lax.all_to_all(jnp.broadcast_to(own_block, (tp_size,) + own_block.shape),...]
    dot_general x0 -> x3, local copies, waits for them, and re-layouts: none -> 5.25 us  [project(): jnp.dot(normed, weight, preferred_element_type=jnp.float32)]
    dot_general x5 -> x4, matrix products: 4.99 us -> 1.39 us  [the longest x1 0.77 us: body(): lax.dot_general(take_map, returned, (((0,), (0,)), ((), ())), preferred_e...]
    dot_general x3, matrix products: 3.35 us -> 1.3 us  [project(): jnp.dot(normed, weight, preferred_element_type=jnp.float32)]
    dot_general x1, matrix products: 2.12 us -> 0.29 us  [body(): jnp.dot(attended.reshape(seq_count, heads_dev * head_dim), w_attn_out, pr...]
  transfers between devices with their start and end apart: 6 -> 4, of which waited for: 4 -> 3; matrix products, arithmetic and copies ran while one was open for 3% -> 18% of each run, Pallas kernels for 0% -> 0%
where the time goes in v1:
time: 79.9 us; the launch traced here: 79.2 us
  waiting for transfers between devices  21.4 us (27%)
  matrix products  18.3 us (23%)
  starting transfers between devices  17.2 us (22%)
  local copies, waits for them, and re-layouts  10.8 us (14%)
  other arithmetic  10.5 us (13%)
  between operations  0.92 us (1%)
    all_to_all x1, waiting for transfers between devices, body(): lax.all_to_all(send_blocks, ('ep', 'tp'), split_axis=0, concat_axis=0, ti...  8.76 us
    all_to_all x1, waiting for transfers between devices, body(): lax.all_to_all(both.reshape(groups, capacity, tp_size, width).transpose(0...  6.86 us
    all_to_all x1, starting transfers between devices, body(): lax.all_to_all(jnp.broadcast_to(own_block, (tp_size,) + own_block.shape),...  6.35 us
    all_to_all x1, waiting for transfers between devices, body(): lax.all_to_all(partial_value.reshape(seq_count, tp_size, width).transpose...  5.78 us
    dot_general x1, matrix products, attend(): jnp.einsum('shd,shld->shl', queries, key_cache, preferred_element_type=jn...  5.65 us
    dot_general x3, local copies, waits for them, and re-layouts, project(): jnp.dot(normed, weight, preferred_element_type=jnp.float32)  5.25 us
    all_to_all x1, starting transfers between devices, body(): lax.all_to_all(partial_value.reshape(seq_count, tp_size, width).transpose...  5.1 us
    dot_general x1, matrix products, attend(): jnp.einsum('shl,shld->shd', weights, value_cache, preferred_element_type=...  4.69 us
  transfers between devices with their start and end apart: 4, of which 3 were waited for; matrix products, arithmetic and copies ran while one was open for 18% of the time, Pallas kernels for 0%

profile of v1, /device:TPU:0, one launch (start us, length us, event | category | flops | bytes accessed | tf_op | source)
XLA Modules:
  0.0 79.2 jit_solution(2475909714023057561)
XLA Ops:
  0.6 0.0 copy-start
  0.7 0.8 reduce-precision_convert_fusion
  1.5 0.7 pad_maximum_fusion
  2.2 0.7 broadcast_in_dim.57
  2.8 6.4 %all-to-all-start = ((bf16[8,24,256]{2,1,0:T(8,128)(2,1)}), bf16[8,24,256]{2,1,0:T(8,128)(2,1)S(1)}, u32[]{:S(2)}, u32[]{:S(2)}) async-start(bf16[8,24,256]{2,1,0:T(8,128)(2,1)} %broadcast_in_dim.57), calls=%async_computation | async-start | bytes 196608 | tf_op jit(solution)/shard_map/all_to_all | solution.py:87
  9.2 0.7 broadcast_add_fusion
  9.8 0.7 iota_compare_fusion.1
  10.6 0.7 mul.194
  11.3 1.5 %copy.162 = bf16[256,2048]{1,0:T(8,128)(2,1)S(1)} copy(bf16[256,2048]{0,1:T(8,128)(2,1)} %bitcast.107) | data formatting | bytes 2097152 | tf_op jit(solution)/shard_map/dot_general | solution.py:102
  12.8 1.5 %copy.163 = bf16[256,2048]{1,0:T(8,128)(2,1)S(1)} copy(bf16[256,2048]{0,1:T(8,128)(2,1)} %bitcast.108) | data formatting | bytes 2097152 | tf_op jit(solution)/shard_map/dot_general | solution.py:102
  14.3 0.1 iota_compare_fusion
  14.3 1.1 %select_reduce_fusion = f32[16,2]{1,0:T(8,128)S(1)} fusion(f32[16,2,1024]{2,1,0:T(2,128)} %param.26, pred[16,1024]{1,0:T(8,128)(4,1)S(1)} %iota_compare_fusion), kind=kLoop, calls=%fused_computation.40 | loop fusion | flops 65504 | bytes 147584 | tf_op jit(solution)/shard_map/reduce_sum | solution.py:114
  15.4 0.1 copy.142
  15.5 2.3 %copy.164 = bf16[256,2048]{1,0:T(8,128)(2,1)} copy(bf16[256,2048]{0,1:T(8,128)(2,1)} %bitcast.109) | data formatting | bytes 2097152 | tf_op jit(solution)/shard_map/dot_general | solution.py:102
  17.8 0.7 fusion.53
  18.6 0.8 %select_reduce_fusion.2 = s32[16]{0:T(128)S(1)} fusion(s32[16,4]{1,0:T(8,128)S(1)} %reduce_window_sum.11, s32[16]{0:T(128)} %bitcast.115), kind=kLoop, calls=%fused_computation.88 | loop fusion | flops 304 | bytes 384 | tf_op jit(solution)/shard_map/reduce_sum | solution.py:143
  19.4 0.7 multiply_add_fusion.1
  20.1 0.8 broadcast_subtract_fusion
  20.8 0.7 dynamic-slice
  21.6 0.7 maximum_multiply_fusion
  22.2 0.1 fusion.12
  22.4 0.1 fusion.25
  22.5 0.5 multiply_reduce_fusion.3
  23.0 0.5 multiply_reduce_fusion.2
  23.5 0.2 fusion.24
  23.7 0.1 fusion.59
  23.8 0.0 copy-start.8
  23.8 0.1 copy.143
  23.9 0.2 multiply_reduce_fusion.1
  24.1 5.7 %fusion.37 = f32[16,2,1,1024]{3,2,1,0:T(1,128)S(1)} fusion(bf16[16,2,1024,128]{3,2,1,0:T(8,128)(2,1)} %param.24, bf16[16,2,128,1]{2,0,1,3:T(8,128)(2,1)S(1)} %get-tuple-element.48), kind=kOutput, calls=%fused_computation.61 | convolution fusion | flops 8388608 | bytes 8527872 | tf_op jit(solution)/shard_map/shd,shld->shl/dot_general | solution.py:28
  29.8 0.0 copy-start.6
  29.8 1.3 %fusion.68 = (f32[16,2]{1,0:T(8,128)S(1)}, f32[16,2,1024]{2,1,0:T(2,128)S(1)}) fusion(f32[16,2,1024]{2,1,0:T(2,128)} %param.26, f32[16,2]{1,0:T(8,128)S(1)} %copy.143, f32[16,2,1,1024]{3,2,1,0:T(1,128)S(1)} %fusion.37, pred[16,1024]{1,0:T(8,128)(4,1)S(1)} %iota_compare_fusion.1), kind=kLoop, calls=%fused_computation.125 | loop fusion | flops 163808 | bytes 409856 | tf_op jit(solution)/shard_map/reduce_max | solution.py:38
  31.1 0.1 copy.145
  31.2 0.1 copy.146
  31.3 0.3 fusion.34
  31.5 0.1 copy.147
  31.6 0.1 copy.148
  31.7 0.3 fusion.28
  32.0 0.4 convolution_convert_fusion.2
  32.4 4.7 %fusion.20 = f32[16,2,1,128]{3,2,1,0:T(1,128)S(1)} fusion(bf16[16,2,1024,128]{3,2,1,0:T(8,128)(2,1)} %param.25, bf16[16,2,1024,1]{2,1,0,3:T(2,128)(2,1)S(1)} %fusion.28), kind=kOutput, calls=%fused_computation.33 | convolution fusion | flops 8388608 | bytes 8470528 | tf_op jit(solution)/shard_map/shl,shld->shd/dot_general | solution.py:44
  37.1 0.3 convolution_convert_fusion
  37.4 0.6 copy.191
  38.0 5.1 %all-to-all-start.1 = ((bf16[8,16,256]{2,1,0:T(8,128)(2,1)}), bf16[8,16,256]{2,1,0:T(8,128)(2,1)S(1)}, u32[]{:S(2)}, u32[]{:S(2)}) async-start(bf16[8,16,256]{2,1,0:T(8,128)(2,1)} %bitcast.96), calls=%async_computation.1 | async-start | bytes 131072 | tf_op jit(solution)/shard_map/all_to_all | solution.py:123
  43.1 0.1 copy.168
  43.2 5.8 %all-to-all-done.1 = bf16[8,16,256]{2,1,0:T(8,128)(2,1)S(1)} async-done(((bf16[8,16,256]{2,1,0:T(8,128)(2,1)}), bf16[8,16,256]{2,1,0:T(8,128)(2,1)S(1)}, u32[]{:S(2)}, u32[]{:S(2)}) %all-to-all-start.1) | async-done | bytes 65568 | tf_op jit(solution)/shard_map/all_to_all | solution.py:123
  49.1 0.1 fusion.4
  49.2 0.7 broadcast_in_dim.99
  49.9 3.1 %all-to-all-start.2 = ((bf16[32,8,384]{2,1,0:T(8,128)(2,1)}), bf16[32,8,384]{2,1,0:T(8,128)(2,1)S(1)}, u32[]{:S(2)}, u32[]{:S(2)}) async-start(bf16[32,8,384]{2,1,0:T(8,128)(2,1)} %bitcast.16), calls=%async_computation.2 | async-start | bytes 393216 | tf_op jit(solution)/shard_map/all_to_all | solution.py:152
  53.1 8.8 %all-to-all-done.2 = bf16[32,8,384]{2,1,0:T(8,128)(2,1)S(1)} async-done(((bf16[32,8,384]{2,1,0:T(8,128)(2,1)}), bf16[32,8,384]{2,1,0:T(8,128)(2,1)S(1)}, u32[]{:S(2)}, u32[]{:S(2)}) %all-to-all-start.2) | async-done | bytes 196640 | tf_op jit(solution)/shard_map/all_to_all | solution.py:152
  61.8 0.1 multiply_reduce_fusion
  62.0 0.1 rsqrt.40
  62.1 0.1 multiply_convert_fusion.1
  62.2 0.1 select_reduce_fusion.1
  62.2 0.1 mul.230
  62.3 0.3 fusion.10
  62.6 0.0 copy-done
  62.6 2.0 %fusion.5 = f32[32,2048]{1,0:T(8,128)S(1)} fusion(bf16[32,2048]{1,0:T(8,128)(2,1)S(1)} %bitcast.105, bf16[1,256,2048]{2,1,0:T(8,128)(2,1)S(1)} %copy-done, bf16[1,2048,256]{2,1,0:T(8,128)(2,1)} %param.41, f32[32,256]{1,0:T(8,128)S(1)} %fusion.10, f32[32]{0:T(128)S(1)} %mul.230), kind=kOutput, calls=%fused_computation.10 | convolution fusion | flops 67166208 | bytes 2523264 | tf_op jit(solution)/shard_map/dot_general | solution.py:173
  64.6 3.0 %fusion.1 = bf16[32,2048]{1,0:T(8,128)(2,1)} fusion(f32[32,2048]{1,0:T(8,128)S(1)} %fusion.5, bf16[256,2048]{1,0:T(8,128)(2,1)} %param.44, f32[2048]{0:T(1024)S(1)} %bitcast.113, bf16[2048,256]{1,0:T(8,128)(2,1)} %param.43, f32[32,2048]{1,0:T(8,128)S(1)} %bitcast.106, f32[2048]{0:T(1024)S(1)} %copy-done.5, f32[32]{0:T(128)S(1)} %rsqrt.40), kind=kOutput, calls=%fused_computation.2 | convolution fusion | flops 67543040 | bytes 2769024 | tf_op jit(solution)/shard_map/dot_general | solution.py:172
  67.6 2.6 %all-to-all-start.3 = ((bf16[32,8,256]{2,1,0:T(8,128)(2,1)}), bf16[32,8,256]{2,1,0:T(8,128)(2,1)S(1)}, u32[]{:S(2)}, u32[]{:S(2)}) async-start(bf16[32,8,256]{2,1,0:T(8,128)(2,1)} %bitcast.28), calls=%async_computation.3 | async-start | bytes 262144 | tf_op jit(solution)/shard_map/all_to_all | solution.py:175
  70.2 0.1 compare_convert_fusion
  70.3 0.6 copy.157
  70.9 0.6 copy.156
  71.5 6.9 %all-to-all-done.3 = bf16[32,8,256]{2,1,0:T(8,128)(2,1)S(1)} async-done(((bf16[32,8,256]{2,1,0:T(8,128)(2,1)}), bf16[32,8,256]{2,1,0:T(8,128)(2,1)S(1)}, u32[]{:S(2)}, u32[]{:S(2)}) %all-to-all-start.3) | async-done | bytes 131104 | tf_op jit(solution)/shard_map/all_to_all | solution.py:175
  78.4 0.8 fusion.6
  (41 shorter events, 0.3 us)
Async XLA Ops:
  0.6 62.0 %copy-start = (bf16[1,256,2048]{2,1,0:T(8,128)(2,1)S(1)}, bf16[1,256,2048]{2,1,0:T(8,128)(2,1)}, u32[]{:S(2)}) copy-start(bf16[1,256,2048]{2,1,0:T(8,128)(2,1)} %param.42) | copy-start | bytes 3145732
  0.6 22.9 %copy-start.7 = (f32[2048]{0:T(1024)S(1)}, f32[2048]{0:T(1024)}, u32[]{:S(2)}) copy-start(f32[2048]{0:T(1024)} %param.28) | copy-start | bytes 24580
  0.7 22.9 %copy-start.4 = (bf16[2048,16]{0,1:T(8,128)(2,1)S(1)}, bf16[2048,16]{0,1:T(8,128)(2,1)}, u32[]{:S(2)}) copy-start(bf16[2048,16]{0,1:T(8,128)(2,1)} %param.32) | copy-start | bytes 196612
  2.8 19.4 %all-to-all-start = ((bf16[8,24,256]{2,1,0:T(8,128)(2,1)}), bf16[8,24,256]{2,1,0:T(8,128)(2,1)S(1)}, u32[]{:S(2)}, u32[]{:S(2)}) async-start(bf16[8,24,256]{2,1,0:T(8,128)(2,1)} %broadcast_in_dim.57), calls=%async_computation | async-start | bytes 196608 | tf_op jit(solution)/shard_map/all_to_all | solution.py:87
  23.0 9.0 %copy-start.1 = (bf16[256,2048]{1,0:T(8,128)(2,1)S(1)}, bf16[256,2048]{1,0:T(8,128)(2,1)}, u32[]{:S(2)}) copy-start(bf16[256,2048]{1,0:T(8,128)(2,1)} %copy.164) | copy-start | bytes 3145732
  23.8 13.2 %copy-start.8 = (f32[16,2]{0,1:T(2,128)}, f32[16,2]{0,1:T(2,128)S(1)}, u32[]{:S(2)}) copy-start(f32[16,2]{0,1:T(2,128)S(1)} %fusion.59) | copy-start | bytes 388
  29.7 7.3 %copy-start.3 = (bf16[256,2048]{1,0:T(8,128)(2,1)S(1)}, bf16[256,2048]{1,0:T(8,128)(2,1)}, u32[]{:S(2)}) copy-start(bf16[256,2048]{1,0:T(8,128)(2,1)} %param.34) | copy-start | bytes 3145732
  29.8 13.3 %copy-start.9 = (s32[16,2]{0,1:T(2,128)S(1)}, s32[16,2]{0,1:T(2,128)}, u32[]{:S(2)}) copy-start(s32[16,2]{0,1:T(2,128)} %param.37) | copy-start | bytes 388
  29.8 13.5 %copy-start.5 = (f32[2048]{0:T(1024)S(1)}, f32[2048]{0:T(1024)}, u32[]{:S(2)}) copy-start(f32[2048]{0:T(1024)} %param.35) | copy-start | bytes 24580
  29.8 19.3 %copy-start.6 = (bf16[16,256]{1,0:T(8,128)(2,1)S(1)}, bf16[16,256]{1,0:T(8,128)(2,1)}, u32[]{:S(2)}) copy-start(bf16[16,256]{1,0:T(8,128)(2,1)} %param.23) | copy-start | bytes 24580
  32.4 30.0 %copy-start.2 = (bf16[1,2048,256]{2,1,0:T(8,128)(2,1)S(1)}, bf16[1,2048,256]{2,1,0:T(8,128)(2,1)}, u32[]{:S(2)}) copy-start(bf16[1,2048,256]{2,1,0:T(8,128)(2,1)} %param.40) | copy-start | bytes 3145732
  38.0 11.0 %all-to-all-start.1 = ((bf16[8,16,256]{2,1,0:T(8,128)(2,1)}), bf16[8,16,256]{2,1,0:T(8,128)(2,1)S(1)}, u32[]{:S(2)}, u32[]{:S(2)}) async-start(bf16[8,16,256]{2,1,0:T(8,128)(2,1)} %bitcast.96), calls=%async_computation.1 | async-start | bytes 131072 | tf_op jit(solution)/shard_map/all_to_all | solution.py:123
  49.9 11.9 %all-to-all-start.2 = ((bf16[32,8,384]{2,1,0:T(8,128)(2,1)}), bf16[32,8,384]{2,1,0:T(8,128)(2,1)S(1)}, u32[]{:S(2)}, u32[]{:S(2)}) async-start(bf16[32,8,384]{2,1,0:T(8,128)(2,1)} %bitcast.16), calls=%async_computation.2 | async-start | bytes 393216 | tf_op jit(solution)/shard_map/all_to_all | solution.py:152
  67.6 10.8 %all-to-all-start.3 = ((bf16[32,8,256]{2,1,0:T(8,128)(2,1)}), bf16[32,8,256]{2,1,0:T(8,128)(2,1)S(1)}, u32[]{:S(2)}, u32[]{:S(2)}) async-start(bf16[32,8,256]{2,1,0:T(8,128)(2,1)} %bitcast.28), calls=%async_computation.3 | async-start | bytes 262144 | tf_op jit(solution)/shard_map/all_to_all | solution.py:175

commit v2 on v1

v2 whole, which is shorter than its diff:
```python
import jax
import jax.numpy as jnp
from jax import lax
from jax.experimental import pallas as pl
from jax.experimental.pallas import tpu as pltpu
from jax.sharding import PartitionSpec as P

FFE = 512
EPG = 4


EPS = 1e-06
FLOOR = -1e30


def norm_rows(row_data, gain_vec):
    values = row_data.astype(jnp.float32)
    factor = lax.rsqrt(jnp.mean(values * values, axis=-1, keepdims=True) + EPS)
    return (values * factor * gain_vec).astype(jnp.bfloat16)


def head_norm(values):
    factor = lax.rsqrt(jnp.mean(values * values, axis=-1, keepdims=True) + EPS)
    return (values * factor).astype(jnp.bfloat16)


def pack_kernel(tokens_ref, gate_ref, out_ref):
    copies, _, width = out_ref.shape
    rows = tokens_ref.shape[0]
    gate = gate_ref[...]
    high = gate.astype(jnp.bfloat16)
    low = (gate - high.astype(jnp.float32)).astype(jnp.bfloat16)
    index = lax.broadcasted_iota(jnp.int32, (8, width), 0)
    extra = jnp.where(
        index == 0, high.astype(jnp.float32), jnp.where(index == 1, low.astype(jnp.float32), 0.0)
    ).astype(jnp.bfloat16)
    tokens = tokens_ref[...]
    for copy in range(copies):
        out_ref[copy, :rows] = tokens
        out_ref[copy, rows:] = extra


def attend_kernel(
    len_smem,
    first_smem,
    x_ref,
    gain_ref,
    len_ref,
    totals_ref,
    wf_ref,
    bias_ref,
    wq_hbm,
    wk_hbm,
    wv_hbm,
    key_hbm,
    value_hbm,
    wo_hbm,
    out_ref,
    new_key_ref,
    new_value_ref,
    new_gate_ref,
    wq,
    wk,
    wv,
    wo,
    keys,
    values,
    score_ref,
    weight_sem,
    key_sem,
    value_sem,
):
    seqs, heads, entries, dim = keys.shape
    chunk = min(256, entries)
    chunks = entries // chunk
    weight_copies = [
        pltpu.make_async_copy(src, dst, weight_sem.at[n])
        for n, (src, dst) in enumerate(
            ((wq_hbm, wq), (wk_hbm, wk), (wv_hbm, wv), (wo_hbm, wo))
        )
    ]

    def cache_copy(src, dst, sem, seq, part):
        cut = pl.ds(0, (part + 1) * chunk)
        return pltpu.make_async_copy(src.at[seq, :, cut, :], dst.at[seq, :, cut, :], sem.at[seq])

    def for_live(action):
        for seq in range(seqs):
            last_part = (len_smem[seq] - 1) // chunk
            for part in range(chunks):
                pl.when(last_part == part)(lambda: action(seq, part))

    for copy in weight_copies[:3]:
        copy.start()
    for_live(lambda seq, part: cache_copy(key_hbm, keys, key_sem, seq, part).start())

    x = x_ref[...].astype(jnp.float32)
    factor = lax.rsqrt(jnp.mean(x * x, axis=-1, keepdims=True) + EPS)
    normed = (x * factor * gain_ref[...]).astype(jnp.bfloat16)
    forget = jnp.dot(normed, wf_ref[...], preferred_element_type=jnp.float32) + bias_ref[...]
    lane = lax.broadcasted_iota(jnp.int32, forget.shape, 1)
    forget_col = jnp.concatenate(
        [
            jnp.sum(jnp.where(lane == first_smem[0] + h, forget, 0.0), axis=1, keepdims=True)
            for h in range(heads)
        ],
        axis=0,
    )
    log_gate = jnp.minimum(forget_col, 0.0) - jnp.log1p(jnp.exp(-jnp.abs(forget_col)))
    totals = totals_ref[...]
    place = lax.broadcasted_iota(jnp.int32, totals.shape, 1)
    length_col = jnp.concatenate([len_ref[...]] * heads, axis=0)
    current = (
        jnp.sum(jnp.where(place == length_col - 1, totals, 0.0), axis=1, keepdims=True) + log_gate
    )
    new_gate_ref[...] = jnp.concatenate(
        [current[h * seqs : (h + 1) * seqs] for h in range(heads)], axis=1
    )
    for seq in range(seqs):
        for part in range(1, chunks):

            @pl.when(part * chunk >= len_smem[seq])
            def _():
                values[seq, :, part * chunk : (part + 1) * chunk, :] = jnp.zeros(
                    (heads, chunk, dim), values.dtype
                )

    def project(n, weight):
        weight_copies[n].wait()
        return jnp.dot(normed, weight[...], preferred_element_type=jnp.float32)

    def head_rows(z):
        return [z[:, h * dim : (h + 1) * dim] for h in range(heads)]

    query_rows = [head_norm(z) for z in head_rows(project(0, wq))]
    key_rows = [head_norm(z) for z in head_rows(project(1, wk))]
    value_rows = [z.astype(jnp.bfloat16) for z in head_rows(project(2, wv))]
    new_key_ref[...] = jnp.concatenate(key_rows, axis=1)
    new_value_ref[...] = jnp.concatenate(value_rows, axis=1)
    for_live(lambda seq, part: cache_copy(value_hbm, values, value_sem, seq, part).start())
    weight_copies[3].start()
    for_live(lambda seq, part: cache_copy(key_hbm, keys, key_sem, seq, part).wait())
    for seq in range(seqs):
        for h in range(heads):
            raw = lax.dot_general(
                query_rows[h],
                keys[seq, h],
                (((1,), (1,)), ((), ())),
                preferred_element_type=jnp.float32,
            )
            score_ref[h * seqs + seq : h * seqs + seq + 1, :] = raw[seq : seq + 1, :]
    scale = dim ** (-0.5)
    live = place < length_col
    scores = jnp.where(live, score_ref[...] * scale + current - totals, FLOOR)
    own_score = (
        jnp.concatenate(
            [
                jnp.sum(q.astype(jnp.float32) * k.astype(jnp.float32), axis=1, keepdims=True)
                for q, k in zip(query_rows, key_rows)
            ],
            axis=0,
        )
        * scale
    )
    peak = jnp.maximum(jnp.max(scores, axis=1, keepdims=True), own_score)
    expo = jnp.where(live, jnp.exp(scores - peak), 0.0)
    own_expo = jnp.exp(own_score - peak)
    denom = jnp.sum(expo, axis=1, keepdims=True) + own_expo
    weights = (expo / denom).astype(jnp.bfloat16)
    own_weight = (own_expo / denom).astype(jnp.bfloat16).astype(jnp.float32)
    for_live(lambda seq, part: cache_copy(value_hbm, values, value_sem, seq, part).wait())
    attended = []
    for h in range(heads):
        head_weights = weights[h * seqs : (h + 1) * seqs]
        for seq in range(seqs):
            mixed = jnp.dot(head_weights, values[seq, h], preferred_element_type=jnp.float32)
            score_ref[h * seqs + seq : h * seqs + seq + 1, :dim] = mixed[seq : seq + 1, :]
        block = slice(h * seqs, (h + 1) * seqs)
        attended.append(
            score_ref[block, :dim] + own_weight[block] * value_rows[h].astype(jnp.float32)
        )
    joined = jnp.concatenate(attended, axis=1).astype(jnp.bfloat16)
    weight_copies[3].wait()
    width = out_ref.shape[2]
    partial = jnp.dot(joined, wo[...], preferred_element_type=jnp.float32).astype(jnp.bfloat16)
    for piece in range(out_ref.shape[0]):
        out_ref[piece] = partial[:, piece * width : (piece + 1) * width]


def branch_kernel(
    expert_smem, recv_ref, gain_ref, gate_ref, wg_hbm, wu_hbm, wi_hbm, wd_hbm, wo_hbm,
    out_ref, wg, wu, wi, wd, wo, rows_ref, route_ref, sems,
):
    copies = [
        pltpu.make_async_copy(src, dst, sems.at[n])
        for n, (src, dst) in enumerate(
            ((wg_hbm.at[0], wg), (wu_hbm.at[0], wu), (wi_hbm, wi), (wd_hbm.at[0], wd), (wo_hbm, wo))
        )
    ]
    for copy in copies:
        copy.start()
    blocks, capacity, wide = recv_ref.shape
    width = wide - 128
    tp_size = rows_ref.shape[1] // width
    for block in range(blocks):
        group, piece = divmod(block, tp_size)
        place = slice(group * capacity, (group + 1) * capacity)
        rows_ref[place, piece * width : (piece + 1) * width] = recv_ref[block, :, :width].astype(
            jnp.float32
        )
        if piece == 0:
            route_ref[place, :] = recv_ref[block, :, width:].astype(jnp.float32)
    lane = lax.broadcasted_iota(jnp.int32, route_ref.shape, 1)
    route = jnp.sum(
        jnp.where(lane == expert_smem[0], route_ref[...], 0.0), axis=1, keepdims=True
    )
    moe_in = norm_rows(rows_ref[...], gain_ref[...])

    def product(n, left, weight):
        copies[n].wait()
        return jnp.dot(left, weight[...], preferred_element_type=jnp.float32)

    gate_pre = product(0, moe_in, wg)
    up_pre = product(1, moe_in, wu)
    hidden = (gate_pre * jax.nn.sigmoid(gate_pre) * up_pre * route).astype(jnp.bfloat16)
    dense_pre = product(2, moe_in, wi)
    dense_hidden = (dense_pre * jax.nn.sigmoid(dense_pre)).astype(jnp.bfloat16)
    expert_part = product(3, hidden, wd)
    dense_part = product(4, dense_hidden, wo)
    both = (expert_part + jax.nn.sigmoid(gate_ref[...]) * dense_part).astype(jnp.bfloat16)
    out_ref[...] = both


def body(
    tokens,
    key_cache,
    value_cache,
    gate_totals,
    lengths,
    attn_gain,
    w_query,
    w_key,
    w_value,
    w_forget,
    forget_bias,
    w_attn_out,
    moe_gain,
    group_ids,
    inner_ids,
    group_prob,
    pair_logits,
    w_expert_gate,
    w_expert_up,
    w_expert_down,
    w_dense_in,
    w_dense_out,
    dense_gate,
):
    tp_size = lax.axis_size("tp")
    groups = lax.axis_size("ep")
    seq_count, width = tokens.shape
    model_dim = width * tp_size
    heads_dev = key_cache.shape[1]
    head_dim = key_cache.shape[3]

    own_block = pl.pallas_call(
        pack_kernel,
        out_shape=jax.ShapeDtypeStruct((tp_size, seq_count + 8, width), jnp.bfloat16),
        name="pack",
    )(tokens, dense_gate[None, :])
    first_recv = lax.all_to_all(
        own_block,
        "tp",
        split_axis=0,
        concat_axis=0,
        tiled=True,
    )
    gathered = first_recv[:, :seq_count].transpose(1, 0, 2).reshape(seq_count, model_dim)
    first_head = lax.axis_index("tp") * heads_dev
    entries = key_cache.shape[2]
    rows = heads_dev * seq_count
    vmem = pl.BlockSpec(memory_space=pltpu.VMEM)
    smem = pl.BlockSpec(memory_space=pltpu.SMEM)
    hbm = pl.BlockSpec(memory_space=pl.ANY)
    blocks_out, new_keys, new_values, new_gates = pl.pallas_call(
        attend_kernel,
        in_specs=[smem, smem] + [vmem] * 6 + [hbm] * 6,
        out_specs=[vmem] * 4,
        out_shape=[
            jax.ShapeDtypeStruct((tp_size, seq_count, width), jnp.bfloat16),
            jax.ShapeDtypeStruct((seq_count, heads_dev * head_dim), jnp.bfloat16),
            jax.ShapeDtypeStruct((seq_count, heads_dev * head_dim), jnp.bfloat16),
            jax.ShapeDtypeStruct((seq_count, heads_dev), jnp.float32),
        ],
        scratch_shapes=[
            pltpu.VMEM(w_query.shape, jnp.bfloat16),
            pltpu.VMEM(w_key.shape, jnp.bfloat16),
            pltpu.VMEM(w_value.shape, jnp.bfloat16),
            pltpu.VMEM(w_attn_out.shape, jnp.bfloat16),
            pltpu.VMEM(key_cache.shape, jnp.bfloat16),
            pltpu.VMEM(value_cache.shape, jnp.bfloat16),
            pltpu.VMEM((rows, entries), jnp.float32),
            pltpu.SemaphoreType.DMA((4,)),
            pltpu.SemaphoreType.DMA((seq_count,)),
            pltpu.SemaphoreType.DMA((seq_count,)),
        ],
        name="attend",
    )(
        lengths,
        first_head.astype(jnp.int32)[None],
        gathered,
        attn_gain[None, :],
        lengths[:, None],
        gate_totals.transpose(1, 0, 2).reshape(rows, entries),
        w_forget,
        forget_bias[None, :],
        w_query,
        w_key,
        w_value,
        key_cache,
        value_cache,
        w_attn_out,
    )
    new_keys = new_keys.reshape(seq_count, heads_dev, head_dim)
    new_values = new_values.reshape(seq_count, heads_dev, head_dim)
    blocks_out, first_recv, group_ids, inner_ids, group_prob, pair_logits = (
        lax.optimization_barrier(
            (blocks_out, first_recv, group_ids, inner_ids, group_prob, pair_logits)
        )
    )
    full_gate = (
        first_recv[:, seq_count].astype(jnp.float32)
        + first_recv[:, seq_count + 1].astype(jnp.float32)
    ).reshape(1, model_dim)
    pieces = lax.all_to_all(
        blocks_out,
        "tp",
        split_axis=0,
        concat_axis=0,
        tiled=True,
    )
    piece_sum = jnp.sum(pieces.astype(jnp.float32), axis=0)
    own_residual = (tokens.astype(jnp.float32) + piece_sum).astype(jnp.bfloat16)

    capacity = max(2, 2 * seq_count // groups)
    first_share = jax.nn.sigmoid(pair_logits[:, 0] - pair_logits[:, 1])
    pair_share = group_prob[:, None] * jnp.stack([first_share, 1.0 - first_share], axis=1)
    inner_range = jnp.arange(EPG)
    spread = jnp.sum(
        jnp.where(inner_ids[:, :, None] == inner_range[None, None, :], pair_share[:, :, None], 0.0),
        axis=1,
    ).astype(jnp.bfloat16)
    choose = (group_ids == jnp.arange(groups)[None, :]).astype(jnp.int32)
    before = jnp.cumsum(choose, axis=0) - choose
    slot_of = group_ids[:, 0] * capacity + jnp.sum(before * choose, axis=1)
    slot_ids = jnp.arange(groups * capacity)
    send_map = (slot_of[None, :] == slot_ids[:, None]).astype(jnp.bfloat16)
    row_data = jnp.concatenate([own_residual, jnp.pad(spread, ((0, 0), (0, 128 - EPG)))], axis=1)
    send_rows = jnp.dot(send_map, row_data, preferred_element_type=jnp.float32).astype(jnp.bfloat16)
    wide = row_data.shape[1]
    send_blocks = jnp.broadcast_to(
        send_rows.reshape(groups, 1, capacity, wide), (groups, tp_size, capacity, wide)
    ).reshape(groups * tp_size, capacity, wide)
    recv_blocks = lax.all_to_all(
        send_blocks, ("ep", "tp"), split_axis=0, concat_axis=0, tiled=True
    )
    expert_index = lax.axis_index("tp") * w_expert_gate.shape[2] // FFE
    both = pl.pallas_call(
        branch_kernel,
        in_specs=[smem] + [vmem] * 3 + [hbm] * 5,
        out_specs=vmem,
        out_shape=jax.ShapeDtypeStruct((groups * capacity, model_dim), jnp.bfloat16),
        scratch_shapes=[
            pltpu.VMEM(w_expert_gate.shape[1:], jnp.bfloat16),
            pltpu.VMEM(w_expert_up.shape[1:], jnp.bfloat16),
            pltpu.VMEM(w_dense_in.shape, jnp.bfloat16),
            pltpu.VMEM(w_expert_down.shape[1:], jnp.bfloat16),
            pltpu.VMEM(w_dense_out.shape, jnp.bfloat16),
            pltpu.VMEM((groups * capacity, model_dim), jnp.float32),
            pltpu.VMEM((groups * capacity, 128), jnp.float32),
            pltpu.SemaphoreType.DMA((5,)),
        ],
        name="branches",
    )(
        expert_index.astype(jnp.int32)[None],
        recv_blocks,
        moe_gain[None, :],
        full_gate,
        w_expert_gate,
        w_expert_up,
        w_dense_in,
        w_expert_down,
        w_dense_out,
    )
    returned = lax.all_to_all(
        both.reshape(groups, capacity, tp_size, width)
        .transpose(0, 2, 1, 3)
        .reshape(groups * tp_size, capacity, width),
        ("ep", "tp"),
        split_axis=0,
        concat_axis=0,
        tiled=True,
    ).reshape(groups * tp_size * capacity, width)
    take_map = jnp.broadcast_to(
        send_map.reshape(groups, 1, capacity, seq_count),
        (groups, tp_size, capacity, seq_count),
    ).reshape(groups * tp_size * capacity, seq_count)
    branch_sum = lax.dot_general(
        take_map, returned, (((0,), (0,)), ((), ())), preferred_element_type=jnp.float32
    )
    layer_output = own_residual.astype(jnp.float32) + branch_sum
    return (layer_output.astype(jnp.bfloat16), new_keys, new_values, new_gates)


def solution(mesh):
    placed = (
        P("ep", "tp"),
        P("ep", "tp", None, None),
        P("ep", "tp", None, None),
        P("ep", "tp", None),
        P("ep"),
        P(),
        P(None, "tp"),
        P(None, "tp"),
        P(None, "tp"),
        P(),
        P(),
        P("tp", None),
        P(),
        P("ep", None),
        P("ep", None),
        P("ep"),
        P("ep", None),
        P("ep", None, "tp"),
        P("ep", None, "tp"),
        P("ep", "tp", None),
        P(None, "tp"),
        P("tp", None),
        P("tp"),
    )
    return jax.shard_map(
        body,
        mesh=mesh,
        in_specs=placed,
        out_specs=(P("ep", "tp"), P("ep", "tp", None), P("ep", "tp", None), P("ep", "tp")),
        check_vma=False,
    )
```

time: 79.9 us -> 66.9 us (0.84)
  matrix products: 18.3 us -> 0.9 us
  Pallas kernels: 0 us -> 17 us
  other arithmetic: 10.5 us -> 1.04 us
  waiting for transfers between devices: 21.4 us -> 19.8 us
  starting transfers between devices: 17.2 us -> 15.8 us
    dot_general x10 -> x0, matrix products: 17.4 us -> none  [the longest x1 5.65 us: attend(): jnp.einsum('shd,shld->shl', queries, key_cache, preferred_element_type=jn...]
    pallas_call x0 -> x3, Pallas kernels: none -> 17 us  [the longest x1 11 us: body(): pl.pallas_call(attend_kernel, in_specs=[smem, smem] + [vmem] * 6 + [hbm]...]
    dot_general x3 -> x0, local copies, waits for them, and re-layouts: 5.25 us -> none  [project(): jnp.dot(normed, weight, preferred_element_type=jnp.float32)]
    all_to_all x1, waiting for transfers between devices: 6.86 us -> 4.13 us  [body(): lax.all_to_all(both.reshape(groups, capacity, tp_size, width).transpose(0...]
    reshape x1 -> x3, local copies, waits for them, and re-layouts: 0.64 us -> 3.24 us  [the longest x1 1.31 us: body(): new_keys = new_keys.reshape(seq_count, heads_dev, head_dim)]
    unnamed x24 -> x16, local copies, waits for them, and re-layouts: 1.38 us -> 3.97 us
    reduce_sum x6 -> x0, other arithmetic: 1.86 us -> none  [the longest x1 1.08 us: body(): new_gates = jnp.sum(jnp.where(at_last, gate_totals, 0.0), axis=2) + log_gate]
    all_to_all x2, waiting for transfers between devices: 5.78 us -> 7.45 us  [the longest x1 5.91 us: body(): lax.all_to_all(blocks_out, 'tp', split_axis=0, concat_axis=0, tiled=True)]
  transfers between devices with their start and end apart: 4 -> 4, of which waited for: 3 -> 4; matrix products, arithmetic and copies ran while one was open for 18% -> 14% of each run, Pallas kernels for 0% -> 0%
where the time goes in v2:
time: 66.9 us; the launch traced here: 66.1 us
  waiting for transfers between devices  19.8 us (30%)
  Pallas kernels  17 us (25%)
  starting transfers between devices  15.8 us (24%)
  local copies, waits for them, and re-layouts  10.8 us (16%)
  other arithmetic  1.04 us (2%)
  matrix products  0.9 us (1%)
  between operations  0.77 us (1%)
    pallas_call x1, Pallas kernels, body(): pl.pallas_call(attend_kernel, in_specs=[smem, smem] + [vmem] * 6 + [hbm]...  11 us
    all_to_all x1, waiting for transfers between devices, body(): lax.all_to_all(send_blocks, ('ep', 'tp'), split_axis=0, concat_axis=0, ti...  8.19 us
    all_to_all x1, starting transfers between devices, body(): lax.all_to_all(own_block, 'tp', split_axis=0, concat_axis=0, tiled=True)  6.35 us
    all_to_all x1, waiting for transfers between devices, body(): lax.all_to_all(blocks_out, 'tp', split_axis=0, concat_axis=0, tiled=True)  5.91 us
    pallas_call x1, Pallas kernels, body(): pl.pallas_call(branch_kernel, in_specs=[smem] + [vmem] * 3 + [hbm] * 5, o...  4.73 us
    all_to_all x1, waiting for transfers between devices, body(): lax.all_to_all(both.reshape(groups, capacity, tp_size, width).transpose(0...  4.13 us
    unnamed x16, local copies, waits for them, and re-layouts  3.97 us
    all_to_all x1, starting transfers between devices, body(): lax.all_to_all(blocks_out, 'tp', split_axis=0, concat_axis=0, tiled=True)  3.58 us
  transfers between devices with their start and end apart: 4, of which 4 were waited for; matrix products, arithmetic and copies ran while one was open for 14% of the time, Pallas kernels for 0%

profile of v2, /device:TPU:0, one launch (start us, length us, event | category | flops | bytes accessed | tf_op | source)
XLA Modules:
  0.0 66.1 jit_solution(15310247039146843346)
XLA Ops:
  0.6 1.3 %pack.1 = bf16[8,24,256]{2,1,0:T(8,128)(2,1)} custom-call(bf16[16,256]{1,0:T(8,128)(2,1)} %tokens_ref.1, f32[1,256]{1,0:T(1,128)} %bitcast.40), custom_call_target="tpu_custom_call" | custom-call | tf_op jit(solution)/shard_map/pack/pallas_call | solution.py:266
  2.0 6.4 %all-to-all-start = ((bf16[8,24,256]{2,1,0:T(8,128)(2,1)}), bf16[8,24,256]{2,1,0:T(8,128)(2,1)S(1)}, u32[]{:S(2)}, u32[]{:S(2)}) async-start(bf16[8,24,256]{2,1,0:T(8,128)(2,1)} %pack.1), calls=%async_computation | async-start | bytes 196608 | tf_op jit(solution)/shard_map/all_to_all | solution.py:271
  8.3 1.8 %copy.43.wf_ref = bf16[2048,16]{1,0:T(8,128)(2,1)} copy(bf16[2048,16]{0,1:T(8,128)(2,1)} %param.32) | data formatting | bytes 131072 | tf_op args[9]
  10.2 1.6 %copy.41 = f32[2,16,1024]{2,1,0:T(8,128)} copy(f32[2,16,1024]{2,0,1:T(2,128)} %bitcast.33) | data formatting | bytes 262144 | tf_op jit(solution)/shard_map/transpose | solution.py:314
  11.8 1.3 %copy.42.len_ref = s32[16,1]{1,0:T(8,128)} copy(s32[16,1]{0,1:T(1,128)} %bitcast.37) | data formatting | bytes 128 | tf_op jit(solution)/shard_map/broadcast_in_dim | solution.py:313
  13.1 1.5 %all-to-all-done = bf16[8,24,256]{2,1,0:T(8,128)(2,1)S(1)} async-done(((bf16[8,24,256]{2,1,0:T(8,128)(2,1)}), bf16[8,24,256]{2,1,0:T(8,128)(2,1)S(1)}, u32[]{:S(2)}, u32[]{:S(2)}) %all-to-all-start) | async-done | bytes 98336 | tf_op jit(solution)/shard_map/all_to_all | solution.py:271
  14.6 0.6 copy.47
  15.3 0.0 copy-start.4
  15.3 0.0 copy-start.5
  15.3 0.0 copy-start.3
  15.3 0.0 copy-start.2
  15.3 0.0 copy-start.1
  15.3 11.0 %attend.1 = (bf16[8,16,256]{2,1,0:T(8,128)(2,1)}, bf16[16,256]{1,0:T(8,128)(2,1)}, bf16[16,256]{1,0:T(8,128)(2,1)}, f32[16,2]{1,0:T(8,128)}) custom-call(s32[16]{0:T(128)} %len_smem.1, s32[1]{0:T(128)} %bitcast.first_smem, bf16[16,2048]{1,0:T(8,128)(2,1)} %bitcast.31, f32[1,2048]{1,0:T(1,128)} %bitcast.35, s32[16,1]{1,0:T(8,128)} %copy.42.len_ref, ...), custom_call_target="tpu_custom_call" | custom-call | tf_op jit(solution)/shard_map/attend/pallas_call | solution.py:285
  26.3 0.0 copy-done.4
  26.3 0.0 copy-done.5
  26.3 0.0 copy-done.3
  26.4 0.1 copy.46
  26.5 0.0 copy-done.2
  26.5 0.1 fusion.10
  26.6 0.2 select_reduce_fusion
  26.8 3.6 %all-to-all-start.1 = ((bf16[8,16,256]{2,1,0:T(8,128)(2,1)}), bf16[8,16,256]{2,1,0:T(8,128)(2,1)S(1)}, u32[]{:S(2)}, u32[]{:S(2)}) async-start(bf16[8,16,256]{2,1,0:T(8,128)(2,1)} %get-tuple-element.15), calls=%async_computation.1 | async-start | bytes 131072 | tf_op jit(solution)/shard_map/all_to_all | solution.py:335
  30.3 5.9 %all-to-all-done.1 = bf16[8,16,256]{2,1,0:T(8,128)(2,1)S(1)} async-done(((bf16[8,16,256]{2,1,0:T(8,128)(2,1)}), bf16[8,16,256]{2,1,0:T(8,128)(2,1)S(1)}, u32[]{:S(2)}, u32[]{:S(2)}) %all-to-all-start.1) | async-done | bytes 65568 | tf_op jit(solution)/shard_map/all_to_all | solution.py:335
  36.3 0.0 copy-done.1
  36.3 0.1 fusion
  36.4 0.7 %broadcast_in_dim.62 = bf16[4,8,8,384]{3,2,1,0:T(8,128)(2,1)} broadcast(bf16[4,8,384]{2,1,0:T(8,128)(2,1)S(1)} %fusion), dimensions={0,2,3} | broadcast | bytes 221184 | tf_op jit(solution)/shard_map/broadcast_in_dim | solution.py:361
  37.1 3.2 %all-to-all-start.2 = ((bf16[32,8,384]{2,1,0:T(8,128)(2,1)}), bf16[32,8,384]{2,1,0:T(8,128)(2,1)S(1)}, u32[]{:S(2)}, u32[]{:S(2)}) async-start(bf16[32,8,384]{2,1,0:T(8,128)(2,1)} %bitcast.12), calls=%async_computation.2 | async-start | bytes 393216 | tf_op jit(solution)/shard_map/all_to_all | solution.py:364
  40.4 0.6 convert_add_fusion
  41.0 8.2 %all-to-all-done.2.recv_ref = bf16[32,8,384]{2,1,0:T(8,128)(2,1)S(1)} async-done(((bf16[32,8,384]{2,1,0:T(8,128)(2,1)}), bf16[32,8,384]{2,1,0:T(8,128)(2,1)S(1)}, u32[]{:S(2)}, u32[]{:S(2)}) %all-to-all-start.2) | async-done | bytes 196640 | tf_op jit(solution)/shard_map/all_to_all | solution.py:364
  49.2 0.0 copy-start
  49.2 0.7 %copy-done = bf16[32,8,384]{2,1,0:T(8,128)(2,1)} copy-done((bf16[32,8,384]{2,1,0:T(8,128)(2,1)}, bf16[32,8,384]{2,1,0:T(8,128)(2,1)S(1)}, u32[]{:S(2)}) %copy-start) | copy-done | bytes 196632
  49.8 4.7 %branches.1 = bf16[32,2048]{1,0:T(8,128)(2,1)} custom-call(s32[1]{0:T(128)} %bitcast.10.expert_smem, bf16[32,8,384]{2,1,0:T(8,128)(2,1)} %copy-done, f32[1,2048]{1,0:T(1,128)} %bitcast.36, f32[1,2048]{1,0:T(1,128)} %bitcast.34, bf16[1,2048,256]{2,1,0:T(8,128)(2,1)} %wg_hbm.1, bf16[1,2048,256]{2,1,0:T(8,128)(2,1)} %wu_hbm.1, bf16[2048,256]{1,0:T(8,128)(2,1)} %wi_hbm.1, ...), custom_call_target="tpu_custom_call" | custom-call | tf_op jit(solution)/shard_map/branches/pallas_call | solution.py:368
  54.6 2.6 %all-to-all-start.3 = ((bf16[32,8,256]{2,1,0:T(8,128)(2,1)}), bf16[32,8,256]{2,1,0:T(8,128)(2,1)S(1)}, u32[]{:S(2)}, u32[]{:S(2)}) async-start(bf16[32,8,256]{2,1,0:T(8,128)(2,1)} %bitcast.30), calls=%async_computation.3 | async-start | bytes 262144 | tf_op jit(solution)/shard_map/all_to_all | solution.py:395
  57.2 1.3 %reshape.129 = bf16[16,2,128]{2,1,0:T(2,128)(2,1)} reshape(bf16[16,256]{1,0:T(8,128)(2,1)} %get-tuple-element.21) | data formatting | bytes 16384 | tf_op jit(solution)/shard_map/reshape | solution.py:324
  58.5 1.3 %reshape.130 = bf16[16,2,128]{2,1,0:T(2,128)(2,1)} reshape(bf16[16,256]{1,0:T(8,128)(2,1)} %get-tuple-element.22) | data formatting | bytes 16384 | tf_op jit(solution)/shard_map/reshape | solution.py:325
  59.8 1.3 %copy.45 = f32[16,2]{0,1:T(2,128)} copy(f32[16,2]{1,0:T(8,128)} %get-tuple-element.35) | data formatting | bytes 256
  61.2 0.1 compare_convert_fusion
  61.2 4.1 %all-to-all-done.3 = bf16[32,8,256]{2,1,0:T(8,128)(2,1)S(1)} async-done(((bf16[32,8,256]{2,1,0:T(8,128)(2,1)}), bf16[32,8,256]{2,1,0:T(8,128)(2,1)S(1)}, u32[]{:S(2)}, u32[]{:S(2)}) %all-to-all-start.3) | async-done | bytes 131104 | tf_op jit(solution)/shard_map/all_to_all | solution.py:395
  65.4 0.8 %fusion.1 = bf16[16,256]{1,0:T(8,128)(2,1)} fusion(bf16[256,16]{1,0:T(8,128)(2,1)S(1)} %bitcast.32, bf16[32,8,256]{2,1,0:T(8,128)(2,1)S(1)} %all-to-all-done.3, bf16[16,256]{1,0:T(8,128)(2,1)S(1)} %add_convert_fusion), kind=kOutput, calls=%fused_computation.3 | convolution fusion | flops 2109440 | bytes 155648 | tf_op jit(solution)/shard_map/dot_general | solution.py:408
  (10 shorter events, 0.1 us)
Async XLA Ops:
  2.0 12.7 %all-to-all-start = ((bf16[8,24,256]{2,1,0:T(8,128)(2,1)}), bf16[8,24,256]{2,1,0:T(8,128)(2,1)S(1)}, u32[]{:S(2)}, u32[]{:S(2)}) async-start(bf16[8,24,256]{2,1,0:T(8,128)(2,1)} %pack.1), calls=%async_computation | async-start | bytes 196608 | tf_op jit(solution)/shard_map/all_to_all | solution.py:271
  15.3 11.0 %copy-start.4 = (f32[16,2]{0,1:T(2,128)S(1)}, f32[16,2]{0,1:T(2,128)}, u32[]{:S(2)}) copy-start(f32[16,2]{0,1:T(2,128)} %param.39) | copy-start | bytes 388
  15.3 11.0 %copy-start.5 = (f32[16]{0:T(128)S(1)}, f32[16]{0:T(128)}, u32[]{:S(2)}) copy-start(f32[16]{0:T(128)} %param.38) | copy-start | bytes 196
  15.3 11.1 %copy-start.3 = (s32[16,2]{0,1:T(2,128)S(1)}, s32[16,2]{0,1:T(2,128)}, u32[]{:S(2)}) copy-start(s32[16,2]{0,1:T(2,128)} %param.37) | copy-start | bytes 388
  15.3 11.2 %copy-start.2 = (s32[16,1]{0,1:T(1,128)S(1)}, s32[16,1]{0,1:T(1,128)}, u32[]{:S(2)}) copy-start(s32[16,1]{0,1:T(1,128)} %param.36) | copy-start | bytes 196
  15.3 21.0 %copy-start.1 = (bf16[16,256]{1,0:T(8,128)(2,1)S(1)}, bf16[16,256]{1,0:T(8,128)(2,1)}, u32[]{:S(2)}) copy-start(bf16[16,256]{1,0:T(8,128)(2,1)} %tokens_ref.1) | copy-start | bytes 24580
  26.8 9.5 %all-to-all-start.1 = ((bf16[8,16,256]{2,1,0:T(8,128)(2,1)}), bf16[8,16,256]{2,1,0:T(8,128)(2,1)S(1)}, u32[]{:S(2)}, u32[]{:S(2)}) async-start(bf16[8,16,256]{2,1,0:T(8,128)(2,1)} %get-tuple-element.15), calls=%async_computation.1 | async-start | bytes 131072 | tf_op jit(solution)/shard_map/all_to_all | solution.py:335
  37.1 12.1 %all-to-all-start.2 = ((bf16[32,8,384]{2,1,0:T(8,128)(2,1)}), bf16[32,8,384]{2,1,0:T(8,128)(2,1)S(1)}, u32[]{:S(2)}, u32[]{:S(2)}) async-start(bf16[32,8,384]{2,1,0:T(8,128)(2,1)} %bitcast.12), calls=%async_computation.2 | async-start | bytes 393216 | tf_op jit(solution)/shard_map/all_to_all | solution.py:364
  49.2 0.7 %copy-start = (bf16[32,8,384]{2,1,0:T(8,128)(2,1)}, bf16[32,8,384]{2,1,0:T(8,128)(2,1)S(1)}, u32[]{:S(2)}) copy-start(bf16[32,8,384]{2,1,0:T(8,128)(2,1)S(1)} %all-to-all-done.2.recv_ref) | copy-start | bytes 589828
  54.6 10.8 %all-to-all-start.3 = ((bf16[32,8,256]{2,1,0:T(8,128)(2,1)}), bf16[32,8,256]{2,1,0:T(8,128)(2,1)S(1)}, u32[]{:S(2)}, u32[]{:S(2)}) async-start(bf16[32,8,256]{2,1,0:T(8,128)(2,1)} %bitcast.30), calls=%async_computation.3 | async-start | bytes 262144 | tf_op jit(solution)/shard_map/all_to_all | solution.py:395
